TPU v7x, 32 devices: a whole 2x2x4 slice. The times are simulated.
32 devices in a mesh: sp: 8 (over z, x), tp: 4 (over y, core).
Axes of the slice: x: 2, y: 2, z: 4, core: 2. Of those that a mesh axis runs over, the one named last changes fastest.
Arguments:
- latents: bfloat16 [4096, 2048], P(('sp', 'tp')), may hold values from -6 to 6
- context: bfloat16 [512, 2048], P('sp'), may hold values from -6 to 6
- cond: float32 [2048], P('sp'), may hold values from -6 to 6
- ctx_cond: float32 [2048], P('sp'), may hold values from -6 to 6
- mod_weight: float32 [2048, 6144], P('sp', 'tp'), may hold values from -0.125 to 0.125
- query_weight: bfloat16 [2048, 2048], P(None, 'tp'), may hold values from -1 to 1, as said below
- key_matrix: bfloat16 [2048, 1024], P(None, 'tp'), may hold values from -1 to 1, as said below
- value_matrix: bfloat16 [2048, 1024], P(None, 'tp'), may hold values from -0.125 to 0.125
- out_weight: bfloat16 [2048, 2048], P('tp'), may hold values from -0.125 to 0.125
- query_gain: float32 [128], replicated, may hold values from 0.7 to 7
- key_gain: float32 [128], replicated, may hold values from 0.7 to 7
Outputs:
- updated: bfloat16 [4096, 2048], P(('sp', 'tp'))
Inputs may be any that keep to these rules, and one draw needn't show every extreme that they name: `query_weight`: entries of order 2048 to the power -1/2. `key_matrix`: entries of order 2048 to the power -1/2.
All inputs are finite; a program needn't handle non-finite values.
Results may differ from a plain program's by a relative error of at most 0.0085.
The roundings to bfloat16 on the way count: a program that leaves them out, or rounds other values in their place, can miss the bound.
Values may be sent and summed in bfloat16 or wider, within the bound.
A program may use at most 128 MiB of HBM per device.

v0:
```python
import math
import jax
import jax.numpy as jnp
from jax import lax
from jax.sharding import PartitionSpec as P

GRID_W = 64
NORM_EPS = 1e-06
ROPE_BASE = 10000.0


def normalize(latent_value_rows):
    return latent_value_rows * lax.rsqrt(
        jnp.mean(latent_value_rows * latent_value_rows, axis=-1, keepdims=True) + NORM_EPS
    )


def rotate(latent_value_rows, positions):
    quarter = latent_value_rows.shape[-1] // 2
    inv_freq = ROPE_BASE ** (-jnp.arange(quarter, dtype=jnp.float32) / quarter)
    angles = positions.astype(jnp.float32)[:, None] * inv_freq[None, :]
    cos_table = jnp.cos(angles)[:, None, :]
    sin_table = jnp.sin(angles)[:, None, :]
    first, second = (latent_value_rows[..., :quarter], latent_value_rows[..., quarter:])
    return jnp.concatenate(
        [first * cos_table - second * sin_table, second * cos_table + first * sin_table], axis=-1
    )


def axial(latent_value_rows, positions):
    half_dim = latent_value_rows.shape[-1] // 2
    return jnp.concatenate(
        [
            rotate(latent_value_rows[..., :half_dim], positions // GRID_W),
            rotate(latent_value_rows[..., half_dim:], positions % GRID_W),
        ],
        axis=-1,
    )


def modulate(latent_value_rows, mod_row):
    model_width = latent_value_rows.shape[-1]
    shift_vec = mod_row[:model_width]
    scale_vec = mod_row[model_width : 2 * model_width]
    return (
        normalize(latent_value_rows.astype(jnp.float32)) * (1.0 + scale_vec) + shift_vec
    ).astype(jnp.bfloat16)


def body(
    latents,
    context,
    cond,
    ctx_cond,
    mod_weight,
    query_weight,
    key_matrix,
    value_matrix,
    out_weight,
    query_gain,
    key_gain,
):
    model_width = latents.shape[1]
    head_dim = query_gain.shape[0]
    sp_count = lax.axis_size("sp")
    partials = jnp.dot(
        jax.nn.silu(jnp.stack([cond, ctx_cond])), mod_weight, precision=lax.Precision.HIGHEST
    )
    summed = lax.psum(partials, "sp")
    modulation = lax.all_gather(summed, "tp", axis=1, tiled=True)
    gate_vec = modulation[0, 2 * model_width :]
    normalised_rows = modulate(latents, modulation[0])
    prefix_normalised = modulate(context, modulation[1])
    query_cols = query_weight.shape[1]
    key_cols = key_matrix.shape[1]
    piece = lax.all_gather(normalised_rows, "tp", axis=0, tiled=True)
    projected = jnp.concatenate(
        [
            jnp.dot(piece, query_weight, preferred_element_type=jnp.float32),
            jnp.dot(piece, key_matrix, preferred_element_type=jnp.float32),
            jnp.dot(piece, value_matrix, preferred_element_type=jnp.float32),
        ],
        axis=1,
    )
    row_count = projected.shape[0]
    positions = lax.axis_index("sp") * row_count + jnp.arange(row_count, dtype=jnp.int32)
    query_heads = projected[:, :query_cols].reshape(row_count, -1, head_dim)
    query_heads = axial(normalize(query_heads) * query_gain, positions).astype(jnp.bfloat16)
    key_heads = projected[:, query_cols : query_cols + key_cols].reshape(row_count, -1, head_dim)
    key_heads = axial(normalize(key_heads) * key_gain, positions).astype(jnp.bfloat16)
    value_heads = (
        projected[:, query_cols + key_cols :].reshape(row_count, -1, head_dim).astype(jnp.bfloat16)
    )
    key_part = jnp.dot(prefix_normalised, key_matrix, preferred_element_type=jnp.float32).reshape(
        prefix_normalised.shape[0], -1, head_dim
    )
    value_part = jnp.dot(
        prefix_normalised, value_matrix, preferred_element_type=jnp.float32
    ).reshape(prefix_normalised.shape[0], -1, head_dim)
    local_keys = (normalize(key_part) * key_gain).astype(jnp.bfloat16)
    local_values = value_part.astype(jnp.bfloat16)
    prefix_keys, prefix_values = (
        lax.all_gather(local_keys, "sp", axis=0, tiled=True),
        lax.all_gather(local_values, "sp", axis=0, tiled=True),
    )
    kv_local = key_heads.shape[1]
    group_size = query_heads.shape[1] // kv_local
    grouped = query_heads.reshape(row_count, kv_local, group_size, head_dim).transpose(1, 2, 0, 3)
    grouped = grouped.reshape(kv_local, group_size * row_count, head_dim)
    inv_root = head_dim ** (-0.5)
    lift = math.log(sp_count * row_count / (2.0 * prefix_keys.shape[0]))
    ctx_scores = (
        jnp.einsum("hqd,khd->hqk", grouped, prefix_keys, preferred_element_type=jnp.float32)
        * inv_root
        + lift
    )
    top_init = jnp.max(ctx_scores, axis=-1)
    ctx_weights = jnp.exp(ctx_scores - top_init[..., None])
    initial = (
        top_init,
        jnp.sum(ctx_weights, axis=-1),
        jnp.einsum(
            "hqk,khd->hqd",
            ctx_weights.astype(jnp.bfloat16),
            prefix_values,
            preferred_element_type=jnp.float32,
        ),
    )

    def update(state_now, key_block, value_block):
        top_old, total_old, acc_old = state_now
        scores = (
            jnp.einsum("hqd,khd->hqk", grouped, key_block, preferred_element_type=jnp.float32)
            * inv_root
        )
        top_new = jnp.maximum(top_old, jnp.max(scores, axis=-1))
        factor = jnp.exp(top_old - top_new)
        weights_now = jnp.exp(scores - top_new[..., None])
        acc_new = acc_old * factor[..., None] + jnp.einsum(
            "hqk,khd->hqd",
            weights_now.astype(jnp.bfloat16),
            value_block,
            preferred_element_type=jnp.float32,
        )
        return (top_new, total_old * factor + jnp.sum(weights_now, axis=-1), acc_new)

    key_piece = lax.all_gather(key_heads, "sp", axis=0, tiled=True)
    value_piece = lax.all_gather(value_heads, "sp", axis=0, tiled=True)
    key_count = key_piece.shape[0]
    rows_per_block = math.gcd(key_count, 2048)
    block_count = key_count // rows_per_block
    key_blocks = key_piece.reshape(block_count, rows_per_block, kv_local, head_dim)
    value_blocks = value_piece.reshape(block_count, rows_per_block, kv_local, head_dim)

    def one_step(state_in, blocks_in):
        return (update(state_in, blocks_in[0], blocks_in[1]), None)

    state_out, _ = lax.scan(one_step, initial, (key_blocks, value_blocks))
    top_fin, total_fin, acc_fin = state_out
    attended = (acc_fin / total_fin[..., None]).astype(jnp.bfloat16)
    attended = (
        attended.reshape(kv_local, group_size, row_count, head_dim)
        .transpose(2, 0, 1, 3)
        .reshape(row_count, -1)
    )
    mixed_rows = lax.psum_scatter(
        jnp.dot(attended, out_weight, preferred_element_type=jnp.float32).astype(jnp.bfloat16),
        "tp",
        scatter_dimension=0,
        tiled=True,
    ).astype(jnp.float32)
    return (latents.astype(jnp.float32) + gate_vec * normalize(mixed_rows)).astype(jnp.bfloat16)


def solution(mesh):
    placed = (
        P(("sp", "tp"), None),
        P("sp", None),
        P("sp"),
        P("sp"),
        P("sp", "tp"),
        P(None, "tp"),
        P(None, "tp"),
        P(None, "tp"),
        P("tp", None),
        P(),
        P(),
    )
    return jax.shard_map(
        body, mesh=mesh, in_specs=placed, out_specs=P(("sp", "tp"), None), check_vma=False
    )
```

profile of v0, /device:TPU:0, one launch (start us, length us, event | category | flops | bytes accessed | tf_op | source)
XLA Modules:
  0.0 286.1 jit_solution(9915169423210026204)
XLA Ops:
  6.5 2.4 fusion.41
  9.0 38.8 %psum.7 = f32[2,1536]{1,0:T(2,128)S(1)} all-reduce(f32[2,1536]{1,0:T(2,128)S(1)} %fusion.41), channel_id=1, replica_groups=mesh['sp'=8,'tp'=4] {'sp'}, use_global_device_ids=true, to_apply=%region_0.1 | all-reduce | flops 3072 | bytes 24576 | tf_op jit(solution)/shard_map/psum | solution.py:69
  47.8 5.2 %all_gather.18 = f32[2,6144]{1,0:T(2,128)S(1)} all-gather(f32[2,1536]{1,0:T(2,128)S(1)} %psum.7), channel_id=1, replica_groups=mesh['sp'=8,'tp'=4] {'tp'}, dimensions={1}, use_global_device_ids=true | all-gather | bytes 61440 | tf_op jit(solution)/shard_map/all_gather | solution.py:70
  53.6 1.2 fusion.27
  54.9 2.1 fusion.30
  59.6 17.4 %all-gather.4.cloned.1.call-done = bf16[512,2048]{1,0:T(8,128)(2,1)} async-done(((bf16[128,2048]{1,0:T(8,128)(2,1)}), bf16[512,2048]{1,0:T(8,128)(2,1)}) %all-gather.4.cloned.1.call-update) | async-done | bytes 2097168 | tf_op jit(solution)/shard_map/all_gather | solution.py:76
  77.0 4.0 %multiply_reduce_fusion.1 = (f32[512,2]{0,1:T(2,128)}, f32[512,256]{0,1:T(8,128)}) fusion(bf16[512,2048]{1,0:T(8,128)(2,1)} %all-gather.4.cloned.1.call-done, bf16[2048,256]{1,0:T(8,128)(2,1)} %param.19), kind=kOutput, calls=%fused_computation.57 | convolution fusion | flops 537132032 | bytes 3674112 | tf_op jit(solution)/shard_map/dot_general | solution.py:80
  81.0 1.3 copy.80
  83.8 1.5 subtract_convert_fusion.1
  87.3 3.3 %convolution_convert_fusion.1 = bf16[512,256]{0,1:T(8,128)(2,1)} fusion(bf16[512,2048]{1,0:T(8,128)(2,1)} %all-gather.4.cloned.1.call-done, bf16[2048,256]{1,0:T(8,128)(2,1)} %param.20), kind=kOutput, calls=%fused_computation.32 | convolution fusion | flops 537001984 | bytes 3407872 | tf_op jit(solution)/shard_map/dot_general | solution.py:81
  90.6 1.8 copy.85
  95.8 1.6 fusion.24
  98.4 31.6 %all_gather.20 = bf16[512,2,128]{2,0,1:T(8,128)(2,1)S(1)} all-gather(bf16[64,2,128]{2,0,1:T(8,128)(2,1)S(1)} %fusion.37), channel_id=1, replica_groups=mesh['sp'=8,'tp'=4] {'sp'}, dimensions={0}, use_global_device_ids=true | all-gather | bytes 294912 | tf_op jit(solution)/shard_map/all_gather | solution.py:103
  129.9 33.5 %all_gather.21 = bf16[512,2,128]{2,0,1:T(8,128)(2,1)} all-gather(bf16[64,2,128]{2,0,1:T(8,128)(2,1)S(1)} %bitcast.103), channel_id=1, replica_groups=mesh['sp'=8,'tp'=4] {'sp'}, dimensions={0}, use_global_device_ids=true | all-gather | bytes 294912 | tf_op jit(solution)/shard_map/all_gather | solution.py:104
  163.5 3.6 %multiply_reduce_fusion = (f32[512,4]{0,1:T(4,128)S(1)}, f32[512,512]{0,1:T(8,128)S(1)}) fusion(bf16[512,2048]{1,0:T(8,128)(2,1)} %all-gather.4.cloned.1.call-done, bf16[2048,512]{1,0:T(8,128)(2,1)} %param.18), kind=kOutput, calls=%fused_computation.44 | convolution fusion | flops 1074264064 | bytes 5251072 | tf_op jit(solution)/shard_map/dot_general | solution.py:79
  169.6 1.9 copy.74
  171.5 1.9 copy.75
  173.5 1.9 pad_maximum_fusion
  177.7 1.2 fusion.19
  179.0 10.1 %all-gather.8.cloned.1.call-done = bf16[4096,2,128]{2,0,1:T(8,128)(2,1)} async-done(((bf16[512,2,128]{2,0,1:T(8,128)(2,1)}), bf16[4096,2,128]{2,0,1:T(8,128)(2,1)}) %all-gather.8.cloned.1.call-update) | async-done | bytes 2097168 | tf_op jit(solution)/shard_map/all_gather | solution.py:148
  189.1 52.1 %while.14 = (s32[]{:T(128)}, f32[2,1024]{1,0:T(2,128)S(1)}, f32[2,1024]{1,0:T(2,128)S(1)}, f32[2,1024,128]{2,1,0:T(8,128)S(1)}, bf16[2,2048,2,128]{3,1,0,2:T(8,1...) while((s32[]{:T(128)}, f32[2,1024]{1,0:T(2,128)S(1)}, ...), condition=%wide.region_11.12_spmd, body=%wide.region_8.11_spmd.sunk | while | flops 2181566464 | bytes 55182420 | solution.py:158
  189.1 9.4 %bitcast_reduce_fusion.2 = (f32[2,1024]{1,0:T(2,128)S(1)}, f32[2,2048,1024]{2,1,0:T(8,128)}) fusion(bf16[2,1024,128]{2,1,0:T(8,128)(2,1)} %get-tuple-element.194, bf16[2,2048,2,128]{3,1,0,2:T(8,128)(2,1)} %get-tuple-element.193, s32[]{:T(128)} %get-tuple-element.181), kind=kOutput, calls=%fused_computation.1.clone.1 | convolution fusion | flops 1082128384 | bytes 18358784 | tf_op jit(solution)/shard_map/while/body/eval_jaxpr/hqd,khd->hqk/dot_general | solution.py:133
  198.5 8.5 %fusion.80 = f32[2,1024]{1,0:T(2,128)S(1)} fusion(f32[2,2048,1024]{2,1,0:T(8,128)} %get-tuple-element.170, f32[2,1024]{1,0:T(2,128)S(1)} %max.4), kind=kLoop, calls=%fused_computation.4.clone.1 | loop fusion | flops 12580864 | bytes 16793600 | tf_op jit(solution)/shard_map/while/body/eval_jaxpr/reduce_sum | solution.py:145
  207.0 8.1 %fusion.81 = f32[2,1024,128]{2,1,0:T(8,128)S(1)} fusion(f32[2,2048,1024]{2,1,0:T(8,128)} %get-tuple-element.170, f32[2,1024]{1,0:T(2,128)S(1)} %max.4, bf16[2,2048,2,128]{3,1,0,2:T(8,128)(2,1)} %get-tuple-element.195, s32[]{:T(128)} %get-tuple-element.181, f32[2,1024,128]{2,1,0:T(8,128)S(1)} %get-tuple-element.184, f32[2,1024]{1,0:T(2,128)S(1)} %get-tuple-element.172), kind=kOutput, calls=%fused_computation.6.clone.1 | convolution fusion | flops 1086849024 | bytes 19939840 | tf_op jit(solution)/shard_map/while/body/eval_jaxpr/hqk,khd->hqd/dot_general | solution.py:139
  215.1 9.4 %bitcast_reduce_fusion.2 = (f32[2,1024]{1,0:T(2,128)S(1)}, f32[2,2048,1024]{2,1,0:T(8,128)}) fusion(bf16[2,1024,128]{2,1,0:T(8,128)(2,1)} %get-tuple-element.194, bf16[2,2048,2,128]{3,1,0,2:T(8,128)(2,1)} %get-tuple-element.193, s32[]{:T(128)} %get-tuple-element.181), kind=kOutput, calls=%fused_computation.1.clone.1 | convolution fusion | flops 1082128384 | bytes 18358784 | tf_op jit(solution)/shard_map/while/body/eval_jaxpr/hqd,khd->hqk/dot_general | solution.py:133
  224.5 8.5 %fusion.80 = f32[2,1024]{1,0:T(2,128)S(1)} fusion(f32[2,2048,1024]{2,1,0:T(8,128)} %get-tuple-element.170, f32[2,1024]{1,0:T(2,128)S(1)} %max.4), kind=kLoop, calls=%fused_computation.4.clone.1 | loop fusion | flops 12580864 | bytes 16793600 | tf_op jit(solution)/shard_map/while/body/eval_jaxpr/reduce_sum | solution.py:145
  233.1 8.1 %fusion.81 = f32[2,1024,128]{2,1,0:T(8,128)S(1)} fusion(f32[2,2048,1024]{2,1,0:T(8,128)} %get-tuple-element.170, f32[2,1024]{1,0:T(2,128)S(1)} %max.4, bf16[2,2048,2,128]{3,1,0,2:T(8,128)(2,1)} %get-tuple-element.195, s32[]{:T(128)} %get-tuple-element.181, f32[2,1024,128]{2,1,0:T(8,128)S(1)} %get-tuple-element.184, f32[2,1024]{1,0:T(2,128)S(1)} %get-tuple-element.172), kind=kOutput, calls=%fused_computation.6.clone.1 | convolution fusion | flops 1086849024 | bytes 19939840 | tf_op jit(solution)/shard_map/while/body/eval_jaxpr/hqk,khd->hqd/dot_general | solution.py:139
  242.3 1.2 copy.88
  243.6 2.6 convolution_convert_fusion
  246.3 29.9 %reduce-scatter.2.cloned.1.call-done = bf16[128,2048]{1,0:T(8,128)(2,1)} async-done(((bf16[512,2048]{1,0:T(8,128)(2,1)}), bf16[128,2048]{1,0:T(8,128)(2,1)}) %reduce-scatter.2.cloned.1.call-update) | async-done | bytes 524304 | tf_op jit(solution)/shard_map/reduce_scatter | solution.py:166
  276.2 1.2 fusion.25
  277.4 2.1 fusion.31
  (71 shorter events, 17.2 us)
Async XLA Ops:
  6.5 237.1 %copy-start = (bf16[512,2048]{1,0:T(8,128)(2,1)S(1)}, bf16[512,2048]{1,0:T(8,128)(2,1)}, u32[]{:S(2)}) copy-start(bf16[512,2048]{1,0:T(8,128)(2,1)} %param.21) | copy-start | bytes 6291460
  6.5 70.5 %all-gather.4.cloned.1.call-start = ((), (), s32[]{:S(2)}) async-start(), calls=%async_computation.1 | async-start | bytes 2621440 | tf_op jit(solution)/shard_map/all_gather | solution.py:76
  57.0 122.0 %all-gather.6.cloned.1.call-start = ((), (), s32[]{:S(2)}) async-start(), calls=%async_computation.2 | async-start | bytes 2359296 | tf_op jit(solution)/shard_map/all_gather | solution.py:147
  57.6 19.4 %copy-start.6 = (f32[512,32]{0,1:T(8,128)}, f32[512,32]{0,1:T(8,128)S(1)}, u32[]{:S(2)}) copy-start(f32[512,32]{0,1:T(8,128)S(1)} %get-tuple-element.112) | copy-start | bytes 196612
  57.6 19.4 %copy-start.8 = (f32[512,32]{0,1:T(8,128)}, f32[512,32]{0,1:T(8,128)S(1)}, u32[]{:S(2)}) copy-start(f32[512,32]{0,1:T(8,128)S(1)} %get-tuple-element.113) | copy-start | bytes 196612
  81.0 5.5 %copy-start.3 = (bf16[64,2048]{1,0:T(8,128)(2,1)S(1)}, bf16[64,2048]{1,0:T(8,128)(2,1)}, u32[]{:S(2)}) copy-start(bf16[64,2048]{1,0:T(8,128)(2,1)} %param.14) | copy-start | bytes 786436
  85.3 8.4 %copy-start.4 = (bf16[2048,256]{1,0:T(8,128)(2,1)S(1)}, bf16[2048,256]{1,0:T(8,128)(2,1)}, u32[]{:S(2)}) copy-start(bf16[2048,256]{1,0:T(8,128)(2,1)} %param.19) | copy-start | bytes 3145732
  86.5 102.6 %all-gather.8.cloned.1.call-start = ((), (), s32[]{:S(2)}) async-start(), calls=%async_computation.3 | async-start | bytes 2359296 | tf_op jit(solution)/shard_map/all_gather | solution.py:148
  92.4 183.8 %reduce-scatter.2.cloned.1.call-start = ((), (), s32[]{:S(2)}) async-start(), calls=%async_computation.4 | async-start | bytes 2621440 | tf_op jit(solution)/shard_map/reduce_scatter | solution.py:166
  93.1 0.6 copy-start.11
  163.4 3.6 %copy-start.12 = (f32[128]{0:T(128)S(1)}, f32[128]{0:T(128)}, u32[]{:S(2)}) copy-start(f32[128]{0:T(128)} %param.22) | copy-start | bytes 1540
  163.4 3.8 %copy-start.7 = (f32[512,32]{0,1:T(8,128)S(1)}, f32[512,32]{0,1:T(8,128)}, u32[]{:S(2)}) copy-start(f32[512,32]{0,1:T(8,128)} %copy-done.6) | copy-start | bytes 196612
  163.4 3.8 %copy-start.9 = (f32[512,32]{0,1:T(8,128)S(1)}, f32[512,32]{0,1:T(8,128)}, u32[]{:S(2)}) copy-start(f32[512,32]{0,1:T(8,128)} %copy-done.8) | copy-start | bytes 196612
  175.3 0.8 copy-start.1
  176.1 1.6 copy-start.5
  243.6 33.8 %copy-start.2 = (bf16[128,2048]{1,0:T(8,128)(2,1)S(1)}, bf16[128,2048]{1,0:T(8,128)(2,1)}, u32[]{:S(2)}) copy-start(bf16[128,2048]{1,0:T(8,128)(2,1)} %param.13) | copy-start | bytes 1572868
  243.6 33.8 %copy-start.10 = (f32[1,2048]{1,0:T(1,128)S(1)}, f32[1,2048]{1,0:T(1,128)}, u32[]{:S(2)}) copy-start(f32[1,2048]{1,0:T(1,128)} %get-tuple-element.103) | copy-start | bytes 24580
Sparse Core Ops, SparseCore 0:
  57.1 19.8 all-gather.3
  86.6 52.3 all-gather.5
  141.2 47.7 all-gather.7
  246.4 29.7 reduce-scatter.1
where the time goes:
time: 287 us; the launch traced here: 286 us
  blocking collectives  109 us (38%)
  waiting for transfers between devices  57.5 us (20%)
  matrix products  55.5 us (19%)
  other arithmetic  36.5 us (13%)
  local copies, waits for them, and re-layouts  13.9 us (5%)
  between operations  13.4 us (5%)
    psum x1, blocking collectives, body(): summed = lax.psum(partials, 'sp')  38.8 us
    all_gather x1, blocking collectives, body(): lax.all_gather(local_values, 'sp', axis=0, tiled=True)  33.5 us
    all_gather x1, blocking collectives, body(): lax.all_gather(local_keys, 'sp', axis=0, tiled=True)  31.6 us
    reduce_scatter x1, waiting for transfers between devices, body(): lax.psum_scatter(jnp.dot(attended, out_weight, preferred_element_type=jnp...  29.9 us
    dot_general x2, matrix products, update(): jnp.einsum('hqd,khd->hqk', grouped, key_block, preferred_element_type=jnp...  18.8 us
    all_gather x1, waiting for transfers between devices, body(): piece = lax.all_gather(normalised_rows, 'tp', axis=0, tiled=True)  17.4 us
    reduce_sum x2, other arithmetic, update(): jnp.sum(weights_now, axis=-1)  17 us
    dot_general x2, matrix products, update(): jnp.einsum('hqk,khd->hqd', weights_now.astype(jnp.bfloat16), value_block,...  16.2 us
  transfers between devices with their start and end apart: 4, of which 3 were waited for; matrix products, arithmetic and copies ran while one was open for 10% of the time, Pallas kernels for 0%

commit v1 on v0

--- a/solution.py
+++ b/solution.py
@@ -73,7 +73,9 @@
     prefix_normalised = modulate(context, modulation[1])
     query_cols = query_weight.shape[1]
     key_cols = key_matrix.shape[1]
-    piece = lax.all_gather(normalised_rows, "tp", axis=0, tiled=True)
+    piece = jnp.concatenate(
+        lax.all_to_all(jnp.stack([normalised_rows] * lax.axis_size("tp")), "tp", 0, 0), axis=0
+    )
     projected = jnp.concatenate(
         [
             jnp.dot(piece, query_weight, preferred_element_type=jnp.float32),

time: 287 us -> 290 us (1.010)
  local copies, waits for them, and re-layouts: 13.9 us -> 22.6 us
  waiting for transfers between devices: 57.5 us -> 52.2 us
  other arithmetic: 36.5 us -> 31.6 us
  starting transfers between devices: 0.13 us -> 4.57 us
    all_to_all x0 -> x1, waiting for transfers between devices: none -> 23 us  [body(): lax.all_to_all(jnp.stack([normalised_rows] * lax.axis_size('tp')), 'tp',...]
    all_gather x1 -> x0, waiting for transfers between devices: 17.4 us -> none  [body(): piece = lax.all_gather(normalised_rows, 'tp', axis=0, tiled=True)]
    all_gather x1, waiting for transfers between devices: 10.1 us -> 0.01 us  [body(): value_piece = lax.all_gather(value_heads, 'sp', axis=0, tiled=True)]
    dot_general x0 -> x3, local copies, waits for them, and re-layouts: none -> 7.68 us  [the longest x1 3.94 us: body(): jnp.dot(piece, query_weight, preferred_element_type=jnp.float32)]
    while x2 -> x3, local copies, waits for them, and re-layouts: 0.01 us -> 6.18 us  [the longest x1 6.17 us: body(): state_out, _ = lax.scan(one_step, initial, (key_blocks, value_blocks))]
    concatenate x4 -> x0, local copies, waits for them, and re-layouts: 5.26 us -> none  [axial(): jnp.concatenate([rotate(latent_value_rows[..., :half_dim], positions // G...]
    all_to_all x0 -> x1, starting transfers between devices: none -> 4.44 us  [body(): lax.all_to_all(jnp.stack([normalised_rows] * lax.axis_size('tp')), 'tp',...]
    reshape x1, local copies, waits for them, and re-layouts: 1.27 us -> 4.67 us  [body(): key_piece.reshape(block_count, rows_per_block, kv_local, head_dim)]
  transfers between devices with their start and end apart: 4 -> 4, of which waited for: 3 -> 2; matrix products, arithmetic and copies ran while one was open for 10% -> 13% of each run, Pallas kernels for 0% -> 0%
where the time goes in v1:
time: 290 us; the launch traced here: 289 us
  blocking collectives  110 us (38%)
  matrix products  54.8 us (19%)
  waiting for transfers between devices  52.2 us (18%)
  other arithmetic  31.6 us (11%)
  local copies, waits for them, and re-layouts  22.6 us (8%)
  between operations  13.4 us (5%)
  starting transfers between devices  4.57 us (2%)
    psum x1, blocking collectives, body(): summed = lax.psum(partials, 'sp')  38.8 us
    all_gather x1, blocking collectives, body(): lax.all_gather(local_values, 'sp', axis=0, tiled=True)  33.4 us
    all_gather x1, blocking collectives, body(): lax.all_gather(local_keys, 'sp', axis=0, tiled=True)  32.3 us
    reduce_scatter x1, waiting for transfers between devices, body(): lax.psum_scatter(jnp.dot(attended, out_weight, preferred_element_type=jnp...  29.1 us
    all_to_all x1, waiting for transfers between devices, body(): lax.all_to_all(jnp.stack([normalised_rows] * lax.axis_size('tp')), 'tp',...  23 us
    dot_general x2, matrix products, update(): jnp.einsum('hqd,khd->hqk', grouped, key_block, preferred_element_type=jnp...  18.8 us
    reduce_sum x2, other arithmetic, update(): jnp.sum(weights_now, axis=-1)  17 us
    dot_general x2, matrix products, update(): jnp.einsum('hqk,khd->hqd', weights_now.astype(jnp.bfloat16), value_block,...  16.2 us
  transfers between devices with their start and end apart: 4, of which 2 were waited for; matrix products, arithmetic and copies ran while one was open for 13% of the time, Pallas kernels for 0%

profile of v1, /device:TPU:0, one launch (start us, length us, event | category | flops | bytes accessed | tf_op | source)
XLA Modules:
  0.0 289.0 jit_solution(6575570806211687196)
XLA Ops:
  6.5 2.4 fusion.41
  9.0 38.8 %psum.7 = f32[2,1536]{1,0:T(2,128)S(1)} all-reduce(f32[2,1536]{1,0:T(2,128)S(1)} %fusion.41), channel_id=1, replica_groups=mesh['sp'=8,'tp'=4] {'sp'}, use_global_device_ids=true, to_apply=%region_0.1 | all-reduce | flops 3072 | bytes 24576 | tf_op jit(solution)/shard_map/psum | solution.py:69
  47.8 5.2 %all_gather.15 = f32[2,6144]{1,0:T(2,128)S(1)} all-gather(f32[2,1536]{1,0:T(2,128)S(1)} %psum.7), channel_id=1, replica_groups=mesh['sp'=8,'tp'=4] {'tp'}, dimensions={1}, use_global_device_ids=true | all-gather | bytes 61440 | tf_op jit(solution)/shard_map/all_gather | solution.py:70
  53.6 1.3 fusion.27
  55.0 1.3 fusion.30
  56.2 1.6 stack.19
  57.8 4.4 %all-to-all-start = ((bf16[4,128,2048]{2,1,0:T(8,128)(2,1)}), bf16[4,128,2048]{2,1,0:T(8,128)(2,1)}, u32[]{:S(2)}, u32[]{:S(2)}) async-start(bf16[4,128,2048]{2,1,0:T(8,128)(2,1)} %stack.19), calls=%async_computation | async-start | bytes 4194304 | tf_op jit(solution)/shard_map/all_to_all | solution.py:77
  62.3 1.4 copy.70
  65.0 23.0 %all-to-all-done = bf16[4,128,2048]{2,1,0:T(8,128)(2,1)} async-done(((bf16[4,128,2048]{2,1,0:T(8,128)(2,1)}), bf16[4,128,2048]{2,1,0:T(8,128)(2,1)}, u32[]{:S(2)}, u32[]{:S(2)}) %all-to-all-start) | async-done | bytes 2097184 | tf_op jit(solution)/shard_map/all_to_all | solution.py:77
  88.0 2.7 multiply_reduce_fusion.1
  92.4 2.3 copy.71
  95.3 3.4 %convolution_convert_fusion.1 = bf16[512,2,128]{2,0,1:T(8,128)(2,1)} fusion(bf16[512,2048,1]{1,0,2:T(8,128)(2,1)} %bitcast.9, bf16[2,128,2048]{2,1,0:T(8,128)(2,1)} %bitcast.102), kind=kOutput, calls=%fused_computation.32 | convolution fusion | flops 537001984 | bytes 3407872 | tf_op jit(solution)/shard_map/dot_general | solution.py:83
  99.9 3.9 %copy.69 = bf16[512,2048]{1,0:T(8,128)(2,1)} copy(bf16[512,2048]{0,1:T(8,128)(2,1)} %bitcast.99) | data formatting | bytes 4194304 | tf_op jit(solution)/shard_map/dot_general | solution.py:81
  103.8 1.6 fusion.39
  106.5 1.6 fusion.24
  109.0 32.3 %all_gather.16 = bf16[512,2,128]{2,0,1:T(8,128)(2,1)S(1)} all-gather(bf16[64,2,128]{2,0,1:T(8,128)(2,1)S(1)} %fusion.37), channel_id=1, replica_groups=mesh['sp'=8,'tp'=4] {'sp'}, dimensions={0}, use_global_device_ids=true | all-gather | bytes 294912 | tf_op jit(solution)/shard_map/all_gather | solution.py:105
  141.3 33.4 %all_gather.17 = bf16[512,2,128]{2,0,1:T(8,128)(2,1)} all-gather(bf16[64,2,128]{2,0,1:T(8,128)(2,1)S(1)} %bitcast.108), channel_id=1, replica_groups=mesh['sp'=8,'tp'=4] {'sp'}, dimensions={0}, use_global_device_ids=true | all-gather | bytes 294912 | tf_op jit(solution)/shard_map/all_gather | solution.py:106
  174.7 3.6 %multiply_reduce_fusion = (f32[512,4]{0,1:T(4,128)S(1)}, f32[512,4,128]{0,2,1:T(8,128)S(1)}) fusion(bf16[512,2048,1]{1,0,2:T(8,128)(2,1)} %bitcast.9, bf16[4,128,2048]{2,1,0:T(8,128)(2,1)} %bitcast.100), kind=kOutput, calls=%fused_computation.44 | convolution fusion | flops 1074264064 | bytes 5251072 | tf_op jit(solution)/shard_map/dot_general | solution.py:81
  181.9 4.7 %reshape.237 = bf16[2,2048,2,128]{1,0,3,2:T(2,128)(2,1)} reshape(bf16[4096,2,128]{0,2,1:T(8,128)(2,1)} %all-gather.3.cloned.1.call-done) | data formatting | bytes 4194304 | tf_op jit(solution)/shard_map/reshape | solution.py:154
  186.6 6.2 %copy.64 = bf16[2,2048,2,128]{3,1,2,0:T(8,128)(2,1)} copy(bf16[2,2048,2,128]{1,0,3,2:T(2,128)(2,1)} %reshape.237) | data formatting | bytes 4194304 | tf_op jit(solution)/shard_map/while | solution.py:160
  192.8 52.1 %while.14 = (s32[]{:T(128)}, f32[2,1024]{1,0:T(2,128)S(1)}, f32[2,1024]{1,0:T(2,128)S(1)}, f32[2,1024,128]{2,1,0:T(8,128)S(1)}, bf16[2,2048,2,128]{3,1,2,0:T(8,1...) while((s32[]{:T(128)}, f32[2,1024]{1,0:T(2,128)S(1)}, ...), condition=%wide.region_11.12_spmd, body=%wide.region_8.11_spmd.sunk | while | flops 2181566464 | bytes 55182420 | solution.py:160
  192.8 9.4 %bitcast_reduce_fusion.2 = (f32[2,1024]{1,0:T(2,128)S(1)}, f32[2,2048,1024]{2,1,0:T(8,128)}) fusion(bf16[2,1024,128]{2,1,0:T(8,128)(2,1)} %get-tuple-element.201, bf16[2,2048,2,128]{3,1,2,0:T(8,128)(2,1)} %get-tuple-element.200, s32[]{:T(128)} %get-tuple-element.188), kind=kOutput, calls=%fused_computation.1.clone.1 | convolution fusion | flops 1082128384 | bytes 18358784 | tf_op jit(solution)/shard_map/while/body/eval_jaxpr/hqd,khd->hqk/dot_general | solution.py:135
  202.2 8.5 %fusion.80 = f32[2,1024]{1,0:T(2,128)S(1)} fusion(f32[2,2048,1024]{2,1,0:T(8,128)} %get-tuple-element.177, f32[2,1024]{1,0:T(2,128)S(1)} %max.4), kind=kLoop, calls=%fused_computation.4.clone.1 | loop fusion | flops 12580864 | bytes 16793600 | tf_op jit(solution)/shard_map/while/body/eval_jaxpr/reduce_sum | solution.py:147
  210.7 8.1 %fusion.81 = f32[2,1024,128]{2,1,0:T(8,128)S(1)} fusion(f32[2,2048,1024]{2,1,0:T(8,128)} %get-tuple-element.177, f32[2,1024]{1,0:T(2,128)S(1)} %max.4, bf16[2,2048,2,128]{3,1,0,2:T(8,128)(2,1)} %get-tuple-element.202, s32[]{:T(128)} %get-tuple-element.188, f32[2,1024,128]{2,1,0:T(8,128)S(1)} %get-tuple-element.191, f32[2,1024]{1,0:T(2,128)S(1)} %get-tuple-element.179), kind=kOutput, calls=%fused_computation.6.clone.1 | convolution fusion | flops 1086849024 | bytes 19939840 | tf_op jit(solution)/shard_map/while/body/eval_jaxpr/hqk,khd->hqd/dot_general | solution.py:141
  218.9 9.4 %bitcast_reduce_fusion.2 = (f32[2,1024]{1,0:T(2,128)S(1)}, f32[2,2048,1024]{2,1,0:T(8,128)}) fusion(bf16[2,1024,128]{2,1,0:T(8,128)(2,1)} %get-tuple-element.201, bf16[2,2048,2,128]{3,1,2,0:T(8,128)(2,1)} %get-tuple-element.200, s32[]{:T(128)} %get-tuple-element.188), kind=kOutput, calls=%fused_computation.1.clone.1 | convolution fusion | flops 1082128384 | bytes 18358784 | tf_op jit(solution)/shard_map/while/body/eval_jaxpr/hqd,khd->hqk/dot_general | solution.py:135
  228.3 8.5 %fusion.80 = f32[2,1024]{1,0:T(2,128)S(1)} fusion(f32[2,2048,1024]{2,1,0:T(8,128)} %get-tuple-element.177, f32[2,1024]{1,0:T(2,128)S(1)} %max.4), kind=kLoop, calls=%fused_computation.4.clone.1 | loop fusion | flops 12580864 | bytes 16793600 | tf_op jit(solution)/shard_map/while/body/eval_jaxpr/reduce_sum | solution.py:147
  236.8 8.1 %fusion.81 = f32[2,1024,128]{2,1,0:T(8,128)S(1)} fusion(f32[2,2048,1024]{2,1,0:T(8,128)} %get-tuple-element.177, f32[2,1024]{1,0:T(2,128)S(1)} %max.4, bf16[2,2048,2,128]{3,1,0,2:T(8,128)(2,1)} %get-tuple-element.202, s32[]{:T(128)} %get-tuple-element.188, f32[2,1024,128]{2,1,0:T(8,128)S(1)} %get-tuple-element.191, f32[2,1024]{1,0:T(2,128)S(1)} %get-tuple-element.179), kind=kOutput, calls=%fused_computation.6.clone.1 | convolution fusion | flops 1086849024 | bytes 19939840 | tf_op jit(solution)/shard_map/while/body/eval_jaxpr/hqk,khd->hqd/dot_general | solution.py:141
  246.1 1.2 copy.66
  247.3 2.6 convolution_convert_fusion
  250.0 29.1 %reduce-scatter.2.cloned.1.call-done = bf16[128,2048]{1,0:T(8,128)(2,1)} async-done(((bf16[512,2048]{1,0:T(8,128)(2,1)}), bf16[128,2048]{1,0:T(8,128)(2,1)}) %reduce-scatter.2.cloned.1.call-update) | async-done | bytes 524304 | tf_op jit(solution)/shard_map/reduce_scatter | solution.py:168
  279.1 1.2 fusion.25
  280.3 2.1 fusion.31
  (65 shorter events, 12.2 us)
Async XLA Ops:
  6.5 240.8 %copy-start = (bf16[512,2048]{1,0:T(8,128)(2,1)S(1)}, bf16[512,2048]{1,0:T(8,128)(2,1)}, u32[]{:S(2)}) copy-start(bf16[512,2048]{1,0:T(8,128)(2,1)} %param.21) | copy-start | bytes 6291460
  53.6 8.7 %copy-start.3 = (bf16[2048,256]{1,0:T(8,128)(2,1)S(1)}, bf16[2048,256]{1,0:T(8,128)(2,1)}, u32[]{:S(2)}) copy-start(bf16[2048,256]{1,0:T(8,128)(2,1)} %param.19) | copy-start | bytes 3145732
  57.8 30.2 %all-to-all-start = ((bf16[4,128,2048]{2,1,0:T(8,128)(2,1)}), bf16[4,128,2048]{2,1,0:T(8,128)(2,1)}, u32[]{:S(2)}, u32[]{:S(2)}) async-start(bf16[4,128,2048]{2,1,0:T(8,128)(2,1)} %stack.19), calls=%async_computation | async-start | bytes 4194304 | tf_op jit(solution)/shard_map/all_to_all | solution.py:77
  62.2 119.7 %all-gather.3.cloned.1.call-start = ((), (), s32[]{:S(2)}) async-start(), calls=%async_computation.2 | async-start | bytes 2359296 | tf_op jit(solution)/shard_map/all_gather | solution.py:149
  88.0 3.5 %copy-start.6 = (f32[512,32]{0,1:T(8,128)S(1)}, f32[512,32]{0,1:T(8,128)}, u32[]{:S(2)}) copy-start(f32[512,32]{0,1:T(8,128)} %get-tuple-element.119) | copy-start | bytes 196612
  88.0 3.5 %copy-start.8 = (f32[512,32]{0,1:T(8,128)S(1)}, f32[512,32]{0,1:T(8,128)}, u32[]{:S(2)}) copy-start(f32[512,32]{0,1:T(8,128)} %get-tuple-element.120) | copy-start | bytes 196612
  88.0 6.7 %copy-start.4 = (bf16[64,2048]{1,0:T(8,128)(2,1)S(1)}, bf16[64,2048]{1,0:T(8,128)(2,1)}, u32[]{:S(2)}) copy-start(bf16[64,2048]{1,0:T(8,128)(2,1)} %param.14) | copy-start | bytes 786436
  92.3 100.5 %all-gather.5.cloned.1.call-start = ((), (), s32[]{:S(2)}) async-start(), calls=%async_computation.3 | async-start | bytes 2359296 | tf_op jit(solution)/shard_map/all_gather | solution.py:150
  98.7 180.4 %reduce-scatter.2.cloned.1.call-start = ((), (), s32[]{:S(2)}) async-start(), calls=%async_computation.4 | async-start | bytes 2621440 | tf_op jit(solution)/shard_map/reduce_scatter | solution.py:168
  141.3 37.0 %copy-start.11 = (f32[128]{0:T(128)S(1)}, f32[128]{0:T(128)}, u32[]{:S(2)}) copy-start(f32[128]{0:T(128)} %param.22) | copy-start | bytes 1540
  174.7 3.8 %copy-start.7 = (f32[512,32]{0,1:T(8,128)S(1)}, f32[512,32]{0,1:T(8,128)}, u32[]{:S(2)}) copy-start(f32[512,32]{0,1:T(8,128)} %get-tuple-element.119) | copy-start | bytes 196612
  174.7 3.8 %copy-start.9 = (f32[512,32]{0,1:T(8,128)S(1)}, f32[512,32]{0,1:T(8,128)}, u32[]{:S(2)}) copy-start(f32[512,32]{0,1:T(8,128)} %get-tuple-element.120) | copy-start | bytes 196612
  179.0 0.8 copy-start.1
  179.0 1.6 copy-start.5
  247.3 33.0 %copy-start.2 = (bf16[128,2048]{1,0:T(8,128)(2,1)S(1)}, bf16[128,2048]{1,0:T(8,128)(2,1)}, u32[]{:S(2)}) copy-start(bf16[128,2048]{1,0:T(8,128)(2,1)} %param.13) | copy-start | bytes 1572868
  247.3 33.0 %copy-start.10 = (f32[1,2048]{1,0:T(1,128)S(1)}, f32[1,2048]{1,0:T(1,128)}, u32[]{:S(2)}) copy-start(f32[1,2048]{1,0:T(1,128)} %get-tuple-element.110) | copy-start | bytes 24580
Sparse Core Ops, SparseCore 0:
  92.4 49.3 all-gather.2
  144.0 47.9 all-gather.4
  250.1 28.9 reduce-scatter.1
